TPU v7x, 32 devices: a whole 2x2x4 slice. The times are simulated.
32 devices in a mesh: kv: 8 (over z, y), tp: 4 (over x, core).
Axes of the slice: x: 2, y: 2, z: 4, core: 2. Of those that a mesh axis runs over, the one named last changes fastest.
Arguments:
- tokens: bfloat16 [32, 6, 2048], replicated, may hold values from -6 to 6
- in_gain: bfloat16 [2048], replicated, may hold values from 0.099609375 to 1.8984375
- w_down_q: bfloat16 [2048, 512], P('kv'), may hold values from -0.125 to 0.125
- w_down_kv: bfloat16 [2048, 256], P('kv'), may hold values from -0.125 to 0.125
- w_rope_key: bfloat16 [2048, 32], replicated, may hold values from -0.125 to 0.125
- q_gain: bfloat16 [512], replicated, may hold values from 0.099609375 to 1.8984375
- kv_gain: bfloat16 [256], replicated, may hold values from 0.099609375 to 1.8984375
- w_up_q: bfloat16 [512, 1536], P(None, 'tp'), may hold values from -0.25 to 0.25
- w_absorb: bfloat16 [16, 64, 256], P('tp'), may hold values from -0.75 to 0.75
- w_value: bfloat16 [256, 1024], P(None, 'tp'), may hold values from -0.375 to 0.375
- w_out: bfloat16 [1024, 2048], P('tp'), may hold values from -0.1875 to 0.1875
- out_gain: bfloat16 [2048], replicated, may hold values from 0.099609375 to 1.8984375
- cache: bfloat16 [32, 16384, 288], P(None, 'kv'), may hold values from -1300 to 1300
- cached: int32 [32], replicated, may hold values from 1 to 16372, as said below
- accepted: int32 [32], replicated, may hold values from 0 to 6
- parents: int32 [32, 6], replicated, may hold values from -1 to 4, as said below
Outputs:
- attended: bfloat16 [32, 6, 2048], P('tp')
- new_cache: bfloat16 [32, 16384, 288], P(None, 'kv')
Inputs may be any that keep to these rules, and one draw needn't show every extreme that they name: Some sequence has at least 15360 cached positions and some has at most 12. parents[s, j] is -1 or less than j.
All inputs are finite; a program needn't handle non-finite values.
Results may differ from a plain program's by a relative error of at most 0.023.
The roundings to bfloat16 on the way count: a program that leaves them out, or rounds other values in their place, can miss the bound.
Values may be sent and summed in bfloat16 or wider, within the bound.
A program may use at most 320 MiB of HBM per device.

v0:
```python
import jax
import jax.numpy as jnp
from jax import lax
from jax.sharding import PartitionSpec as P

EPSILON = 1e-06
ROTARY_BASE = 10000.0
FLOOR_SCORE = -1e30


def joined(value, axis, join):
    pieces = jax.tree.map(lambda part: lax.all_gather(part, axis), value)
    head = jax.tree.map(lambda part: part[0], pieces)
    tail = jax.tree.map(lambda part: part[1:], pieces)
    total, _ = lax.scan(lambda total, section: (join(total, section), None), head, tail)
    return total


def rms_scale(values, gain_vec):
    floats = values.astype(jnp.float32)
    return (
        floats
        * lax.rsqrt(jnp.mean(floats * floats, axis=-1, keepdims=True) + EPSILON)
        * gain_vec.astype(jnp.float32)
    )


def rotate(values, positions):
    half_width = values.shape[-1] // 2
    frequency = ROTARY_BASE ** (-jnp.arange(half_width, dtype=jnp.float32) * 2.0 / values.shape[-1])
    angles = positions.astype(jnp.float32)[..., None] * frequency
    cosine = jnp.cos(angles)
    sine_part = jnp.sin(angles)
    lower_half = values[..., :half_width]
    upper_half = values[..., half_width:]
    return jnp.concatenate(
        [
            lower_half * cosine - upper_half * sine_part,
            lower_half * sine_part + upper_half * cosine,
        ],
        axis=-1,
    )


def ancestry(parents):
    num_prop = parents.shape[-1]
    slot_ids = jnp.arange(num_prop, dtype=jnp.int32)
    parent_hot = parents[:, :, None] == slot_ids[None, None, :]
    itself_mask = jnp.broadcast_to(slot_ids[:, None] == slot_ids[None, :], parent_hot.shape)
    reached = itself_mask
    for repeat in range(num_prop):
        reached = itself_mask | jnp.any(parent_hot[:, :, :, None] & reached[:, None, :, :], axis=2)
    return reached


def combine_totals(earlier, later_part):
    peak_left, denom_left, numer_left = earlier
    peak_right, denom_right, numer_right = later_part
    highest = jnp.maximum(peak_left, peak_right)
    factor_left = jnp.exp(peak_left - highest)
    factor_right = jnp.exp(peak_right - highest)
    return (
        highest,
        denom_left * factor_left + denom_right * factor_right,
        numer_left * factor_left[..., None] + numer_right * factor_right[..., None],
    )


def finish_latent(top_score, denominator, numerator, prop_peak, prop_den, prop_num):
    highest_all = jnp.maximum(top_score, prop_peak)
    cache_factor = jnp.exp(top_score - highest_all)
    prop_factor = jnp.exp(prop_peak - highest_all)
    return (
        (numerator * cache_factor[..., None] + prop_num * prop_factor[..., None])
        / (denominator * cache_factor + prop_den * prop_factor)[..., None]
    ).astype(jnp.bfloat16)


def local(
    tokens,
    in_gain,
    w_down_q,
    w_down_kv,
    w_rope_key,
    q_gain,
    kv_gain,
    w_up_q,
    w_absorb,
    w_value,
    w_out,
    out_gain,
    cache,
    cached,
    accepted,
    parents,
):
    f32 = jnp.float32
    bf16 = jnp.bfloat16
    num_seqs = tokens.shape[0]
    num_prop = tokens.shape[1]
    model_width = tokens.shape[2]
    num_rows = num_seqs * num_prop
    down_rows = w_down_q.shape[0]
    latent_width = w_down_kv.shape[1]
    rope_width = w_rope_key.shape[1]
    local_heads = w_absorb.shape[0]
    nope_width = w_absorb.shape[1]
    value_width = w_value.shape[1] // local_heads
    local_span = cache.shape[1]
    normed = rms_scale(tokens, in_gain).astype(bf16).reshape(num_rows, model_width)
    own_cols = lax.dynamic_slice_in_dim(normed, lax.axis_index("kv") * down_rows, down_rows, 1)
    part_query = jnp.dot(own_cols, w_down_q, preferred_element_type=f32)
    part_latent = jnp.dot(own_cols, w_down_kv, preferred_element_type=f32)
    sum_query, sum_latent = lax.psum((part_query, part_latent), "kv")
    query_in = rms_scale(sum_query, q_gain).astype(bf16)
    latent = rms_scale(sum_latent, kv_gain).astype(bf16)
    lengths = cached + accepted
    reached = ancestry(parents)
    depth_of = jnp.sum(reached.astype(jnp.int32), axis=-1) - 1
    positions = lengths[:, None] + depth_of
    rope_key = rotate(
        jnp.dot(normed, w_rope_key, preferred_element_type=f32).reshape(
            num_seqs, num_prop, rope_width
        ),
        positions,
    ).astype(bf16)
    latent_rows = latent.reshape(num_seqs, num_prop, latent_width)
    new_rows = jnp.concatenate([latent_rows, rope_key], axis=-1)
    queries = jnp.dot(query_in, w_up_q, preferred_element_type=f32).reshape(
        num_seqs, num_prop, local_heads, nope_width + rope_width
    )
    query_nope = queries[..., :nope_width].astype(bf16)
    query_rope = rotate(queries[..., nope_width:], positions[:, :, None]).astype(bf16)
    query_lat = jnp.einsum(
        "sphn,hnc->sphc", query_nope, w_absorb, preferred_element_type=f32
    ).astype(bf16)
    full_query = jnp.concatenate([query_lat, query_rope], axis=-1)
    score_scale = (nope_width + rope_width) ** (-0.5)
    offset = lax.axis_index("kv") * local_span
    key_pos = offset + jnp.arange(local_span, dtype=jnp.int32)
    visible = key_pos[None, :] < lengths[:, None]
    flat_query = full_query.reshape(num_seqs, num_prop * local_heads, latent_width + rope_width)
    scores = jnp.einsum("sjc,skc->sjk", flat_query, cache, preferred_element_type=f32) * score_scale
    masked = jnp.where(visible[:, None, :], scores, FLOOR_SCORE)
    top_score = jnp.max(masked, axis=-1)
    weights = jnp.where(visible[:, None, :], jnp.exp(masked - top_score[..., None]), 0.0)
    denominator = jnp.sum(weights, axis=-1)
    numerator = jnp.einsum(
        "sjk,skc->sjc", weights.astype(bf16), cache[:, :, :latent_width], preferred_element_type=f32
    )
    prop_scores = (
        jnp.einsum("sphc,skc->sphk", full_query, new_rows, preferred_element_type=f32) * score_scale
    )
    allowed = reached[:, :, None, :]
    prop_masked = jnp.where(allowed, prop_scores, FLOOR_SCORE)
    prop_peak = jnp.max(prop_masked, axis=-1)
    prop_weights = jnp.where(allowed, jnp.exp(prop_masked - prop_peak[..., None]), 0.0)
    prop_den = jnp.sum(prop_weights, axis=-1)
    prop_num = jnp.einsum(
        "sphk,skc->sphc", prop_weights.astype(bf16), latent_rows, preferred_element_type=f32
    )
    top_score, denominator, numerator = joined(
        (top_score, denominator, numerator), "kv", combine_totals
    )
    lat_out = finish_latent(
        top_score.reshape(num_seqs, num_prop, local_heads),
        denominator.reshape(num_seqs, num_prop, local_heads),
        numerator.reshape(num_seqs, num_prop, local_heads, latent_width),
        prop_peak,
        prop_den,
        prop_num,
    )
    head_out = jnp.einsum(
        "sphc,chv->sphv",
        lat_out,
        w_value.reshape(latent_width, local_heads, value_width),
        preferred_element_type=f32,
    ).astype(bf16)
    head_out = head_out.reshape(num_seqs, num_prop, local_heads * value_width)
    summed = lax.psum_scatter(
        jnp.dot(
            head_out.reshape(
                num_seqs // lax.axis_size("tp") * lax.axis_size("tp") * num_prop,
                local_heads * value_width,
            ),
            w_out,
            preferred_element_type=f32,
        )
        .reshape(num_seqs // lax.axis_size("tp") * lax.axis_size("tp"), num_prop, model_width)
        .astype(jnp.bfloat16),
        "tp",
        scatter_dimension=0,
        tiled=True,
    ).astype(jnp.float32)
    attended = rms_scale(summed, out_gain).astype(bf16)
    local_slots = lengths[:, None] + jnp.arange(num_prop, dtype=jnp.int32)[None, :] - offset
    on_shard = (local_slots >= 0) & (local_slots < local_span)
    target = jnp.where(on_shard, local_slots, local_span)
    seq_ids = jnp.broadcast_to(jnp.arange(num_seqs, dtype=jnp.int32)[:, None], target.shape)
    new_cache = cache.at[seq_ids, target].set(new_rows, mode="drop")
    return (attended, new_cache)


def solution(mesh):
    placed = (
        P(),
        P(),
        P("kv", None),
        P("kv", None),
        P(),
        P(),
        P(),
        P(None, "tp"),
        P("tp", None, None),
        P(None, "tp"),
        P("tp", None),
        P(),
        P(None, "kv", None),
        P(),
        P(),
        P(),
    )
    return jax.shard_map(
        local,
        mesh=mesh,
        in_specs=placed,
        out_specs=(P("tp", None, None), P(None, "kv", None)),
        check_vma=False,
    )
```

profile of v0, /device:TPU:0, one launch (start us, length us, event | category | flops | bytes accessed | tf_op | source)
XLA Modules:
  0.0 340.1 jit_solution(10780323877964826373)
XLA Ops:
  7.3 0.9 convert_element_type.75
  8.1 1.4 fusion.15
  9.5 1.4 fusion.17
  10.9 0.4 copy.179
  11.4 1.1 reshape.287
  12.5 2.0 fusion.42
  14.5 1.8 fusion.40
  16.3 0.7 fusion.38
  17.1 0.1 and_reduce_fusion.5
  17.8 0.1 convert_reduce_fusion
  17.9 0.3 subtract_convert_fusion.1
  18.3 0.1 copy.184
  18.4 55.0 %copy.191 = bf16[32,2048,288]{2,1,0:T(8,128)(2,1)} copy(bf16[32,2048,288]{1,2,0:T(8,128)(2,1)} %param.30) | data formatting | bytes 75497472 | tf_op args[12]
  73.4 0.1 broadcast_compare_fusion
  73.5 18.9 %all-reduce.3.cloned.1.call-done = (f32[192,512]{1,0:T(8,128)}, f32[192,256]{1,0:T(8,128)}) async-done(((f32[192,512]{1,0:T(8,128)}, f32[192,256]{1,0:T(8,128)}), (f32[192,512]{1,0:T(8,128)}, f32[192,256]{1,0:T(8,128)})) %all-reduce.3.cloned.1.call-update) | async-done | bytes 589840 | tf_op jit(solution)/shard_map/psum | solution.py:114
  92.4 1.1 multiply_reduce_fusion
  93.6 1.3 fusion.32
  94.9 0.3 reshape.288
  95.1 0.5 fusion.64
  95.7 0.2 fusion.21
  95.9 0.2 subtract_convert_fusion
  96.1 0.1 pad_maximum_fusion
  96.3 17.9 %fusion.5 = (f32[32,24]{1,0:T(8,128)S(1)}, f32[32,24,2048]{2,1,0:T(8,128)}) fusion(pred[32,2048]{1,0:T(8,128)(4,1)S(1)} %broadcast_compare_fusion, bf16[32,2048,288]{1,2,0:T(8,128)(2,1)} %param.30, bf16[32,24,288]{2,0,1:T(8,128)(2,1)S(1)} %bitcast.84), kind=kOutput, calls=%fused_computation.13 | convolution fusion | flops 910687488 | bytes 44551168 | tf_op jit(solution)/shard_map/sjc,skc->sjk/dot_general | solution.py:143
  114.2 16.2 %fusion.3 = f32[32,24,256]{2,1,0:T(8,128)} fusion(bf16[32,2048,288]{2,1,0:T(8,128)(2,1)} %copy.191, f32[32,24,2048]{2,1,0:T(8,128)} %get-tuple-element.90, f32[32,24]{1,0:T(8,128)S(1)} %get-tuple-element.89, pred[32,2048]{1,0:T(8,128)(4,1)S(1)} %broadcast_compare_fusion), kind=kOutput, calls=%fused_computation.9 | convolution fusion | flops 813170688 | bytes 40700928 | tf_op jit(solution)/shard_map/sjk,skc->sjc/dot_general | solution.py:148
  130.5 0.2 reduce-scatter.4.cloned.1.call-start
  130.7 0.8 copy.202
  131.5 0.1 copy.194
  131.6 0.1 copy.193
  131.8 0.1 multiply_reduce_fusion.1
  131.9 0.1 multiply_convert_fusion.2
  132.1 0.1 pad_maximum_fusion.1
  132.2 2.4 fusion.24
  134.6 0.3 copy.196
  135.1 0.5 copy.199
  135.7 4.3 %fusion.7 = f32[32,24]{1,0:T(8,128)S(1)} fusion(f32[32,24,2048]{2,1,0:T(8,128)} %get-tuple-element.90, f32[32,24]{1,0:T(8,128)S(1)} %get-tuple-element.89, pred[32,2048]{1,0:T(8,128)(4,1)S(1)} %broadcast_compare_fusion), kind=kLoop, calls=%fused_computation.15 | loop fusion | flops 7863552 | bytes 6363136 | tf_op jit(solution)/shard_map/reduce_sum | solution.py:147
  140.1 31.9 %all-gather.3 = f32[8,32,24]{1,2,0:T(8,128)S(1)} all-gather(f32[1,32,24]{1,2,0:T(8,128)S(1)} %copy.189), channel_id=2, replica_groups=mesh['kv'=8,'tp'=4] {'kv'}, dimensions={0}, use_global_device_ids=true | all-gather | bytes 27648 | tf_op jit(solution)/shard_map/all_gather | solution.py:12
  172.0 32.1 %all-gather.4 = f32[8,32,24]{1,2,0:T(8,128)S(1)} all-gather(f32[1,32,24]{1,2,0:T(8,128)S(1)} %copy.190), channel_id=3, replica_groups=mesh['kv'=8,'tp'=4] {'kv'}, dimensions={0}, use_global_device_ids=true | all-gather | bytes 27648 | tf_op jit(solution)/shard_map/all_gather | solution.py:12
  204.1 26.5 %all-gather.7.cloned.1.call-done = f32[256,24,256]{2,1,0:T(8,128)} async-done(((f32[32,24,256]{2,1,0:T(8,128)}), f32[256,24,256]{2,1,0:T(8,128)}) %all-gather.7.cloned.1.call-update) | async-done | bytes 6291472 | tf_op jit(solution)/shard_map/all_gather | solution.py:12
  230.6 5.4 %slice.73 = f32[224,24,256]{2,1,0:T(8,128)} slice(f32[256,24,256]{2,1,0:T(8,128)} %all-gather.7.cloned.1.call-done), slice={[32:256], [0:24], [0:256]} | slice | bytes 11010048 | tf_op jit(solution)/shard_map/slice | solution.py:14
  236.0 11.5 %while.14 = (s32[]{:T(128)}, f32[32,24]{0,1:T(8,128)S(1)}, f32[32,24]{0,1:T(8,128)S(1)}, f32[32,24,256]{2,1,0:T(8,128)S(1)}, f32[7,32,24]{1,2,0:T(8,128)S(1)}, /...) while((s32[]{:T(128)}, f32[32,24]{0,1:T(8,128)S(1)}, f32[32,24]{0,1:T(8,128)S(1)}, ...), condition=%wide.region_13.14_spmd, body=%wide.region_12.13_spmd.sunk | while | flops 594434 | bytes 2402405 | solution.py:15
  236.2 1.5 fusion.76
  237.9 1.5 fusion.76
  239.5 1.5 fusion.76
  241.2 1.5 fusion.76
  242.8 1.5 fusion.76
  244.5 1.5 fusion.76
  246.1 1.5 fusion.76
  247.6 0.3 copy.192
  247.9 0.1 copy.201
  248.0 0.1 copy.200
  248.1 0.1 copy.197
  248.2 0.8 fusion.20
  249.0 0.4 fusion.22
  249.4 0.2 copy.204
  249.6 0.2 dot_general.45
  249.7 0.4 fusion.14
  250.1 1.0 copy.217
  251.2 0.1 fusion.49
  251.3 0.1 reshape.295
  251.4 0.1 reshape.297
  251.5 25.0 %scatter_fusion = bf16[32,2048,288]{2,1,0:T(8,128)(2,1)} fusion(bf16[32,2048,288]{2,1,0:T(8,128)(2,1)} %copy.191, s32[192]{0:T(256)S(1)} %reshape.295, bf16[192,288]{1,0:T(8,128)(2,1)S(1)} %reshape.297), kind=kCustom, calls=%fused_computation | custom fusion | bytes 333312 | tf_op jit(solution)/shard_map/scatter | solution.py:200
  276.5 54.3 %copy.206 = bf16[32,2048,288]{1,2,0:T(8,128)(2,1)} copy(bf16[32,2048,288]{2,1,0:T(8,128)(2,1)} %scatter_fusion) | data formatting | bytes 75497472
  330.8 1.0 fusion.28
  331.9 1.7 fusion.30
  (94 shorter events, 2.6 us)
Async XLA Ops:
  7.2 242.6 %copy-start = (bf16[256,2048]{1,0:T(8,128)(2,1)S(1)}, bf16[256,2048]{1,0:T(8,128)(2,1)}, u32[]{:S(2)}) copy-start(bf16[256,2048]{1,0:T(8,128)(2,1)} %param.28) | copy-start | bytes 3145732
  7.2 7.3 %copy-start.5 = (bf16[256,256]{1,0:T(8,128)(2,1)S(1)}, bf16[256,256]{1,0:T(8,128)(2,1)}, u32[]{:S(2)}) copy-start(bf16[256,256]{1,0:T(8,128)(2,1)} %param.21) | copy-start | bytes 393220
  7.2 9.1 %copy-start.7 = (bf16[2048,32]{0,1:T(8,128)(2,1)S(1)}, bf16[2048,32]{0,1:T(8,128)(2,1)}, u32[]{:S(2)}) copy-start(bf16[2048,32]{0,1:T(8,128)(2,1)} %param.22) | copy-start | bytes 393220
  7.2 9.9 %copy-start.9 = (s32[32,6]{0,1:T(8,128)S(1)}, s32[32,6]{0,1:T(8,128)}, u32[]{:S(2)}) copy-start(s32[32,6]{0,1:T(8,128)} %param.33) | copy-start | bytes 2308
  7.2 10.6 %copy-start.11 = (s32[32]{0:T(128)S(1)}, s32[32]{0:T(128)}, u32[]{:S(2)}) copy-start(s32[32]{0:T(128)} %param.31) | copy-start | bytes 388
  7.2 10.6 %copy-start.12 = (s32[32]{0:T(128)S(1)}, s32[32]{0:T(128)}, u32[]{:S(2)}) copy-start(s32[32]{0:T(128)} %param.32) | copy-start | bytes 388
  7.2 10.9 %copy-start.10 = (bf16[512]{0:T(512)(128)(2,1)S(1)}, bf16[512]{0:T(512)(128)(2,1)}, u32[]{:S(2)}) copy-start(bf16[512]{0:T(512)(128)(2,1)} %param.23) | copy-start | bytes 3076
  7.2 85.2 %all-reduce.3.cloned.1.call-start = ((), (), s32[]{:S(2)}) async-start(), calls=%async_computation.3 | async-start | bytes 1179648 | tf_op jit(solution)/shard_map/psum | solution.py:114
  16.2 214.4 %all-gather.7.cloned.1.call-start = ((), (), s32[]{:S(2)}) async-start(), calls=%async_computation.1 | async-start | bytes 7077888 | tf_op jit(solution)/shard_map/all_gather | solution.py:12
  18.4 75.2 %copy-start.2 = (bf16[512,384]{1,0:T(8,128)(2,1)S(1)}, bf16[512,384]{1,0:T(8,128)(2,1)}, u32[]{:S(2)}) copy-start(bf16[512,384]{1,0:T(8,128)(2,1)} %param.25) | copy-start | bytes 1179652
  18.4 77.3 %copy-start.6 = (bf16[4,64,256]{2,1,0:T(8,128)(2,1)S(1)}, bf16[4,64,256]{2,1,0:T(8,128)(2,1)}, u32[]{:S(2)}) copy-start(bf16[4,64,256]{2,1,0:T(8,128)(2,1)} %param.26) | copy-start | bytes 393220
  114.2 16.5 %copy-start.3 = (bf16[256,256]{1,0:T(8,128)(2,1)S(1)}, bf16[256,256]{1,0:T(8,128)(2,1)}, u32[]{:S(2)}) copy-start(bf16[256,256]{1,0:T(8,128)(2,1)} %param.27) | copy-start | bytes 393220
  114.2 17.5 %copy-start.13 = (bf16[256]{0:T(256)(128)(2,1)S(1)}, bf16[256]{0:T(256)(128)(2,1)}, u32[]{:S(2)}) copy-start(bf16[256]{0:T(256)(128)(2,1)} %param.24) | copy-start | bytes 1540
  114.2 17.5 %copy-start.1 = (f32[192,256]{1,0:T(8,128)S(1)}, f32[192,256]{1,0:T(8,128)}, u32[]{:S(2)}) copy-start(f32[192,256]{1,0:T(8,128)} %get-tuple-element.69) | copy-start | bytes 589828
  130.5 200.3 %reduce-scatter.4.cloned.1.call-start = ((), (), s32[]{:S(2)}) async-start(), calls=%async_computation.2 | async-start | bytes 983040
  230.6 5.4 %slice-start = ((f32[256,24,256]{2,1,0:T(8,128)}), f32[32,24,256]{2,1,0:T(8,128)S(1)}, s32[]{:S(2)}) async-start(f32[256,24,256]{2,1,0:T(8,128)} %all-gather.7.cloned.1.call-done), calls=%async_computation.4 | async-start | bytes 1572864 | tf_op jit(solution)/shard_map/slice | solution.py:13
  247.6 1.4 copy-start.4
  247.8 3.3 copy-start.8
Sparse Core Ops, SparseCore 0:
  16.4 76.0 all-reduce.2
  130.6 99.9 all-gather.6
  251.3 21.5 reduce-scatter.3
where the time goes:
time: 344 us; the launch traced here: 340 us
  local copies, waits for them, and re-layouts  148 us (43%)
  blocking collectives  64 us (19%)
  waiting for transfers between devices  45.5 us (13%)
  matrix products  44.1 us (13%)
  other arithmetic  24.2 us (7%)
  between operations  14.3 us (4%)
    unnamed x34, local copies, waits for them, and re-layouts  111 us
    all_gather x2, blocking collectives, joined(): pieces = jax.tree.map(lambda part: lax.all_gather(part, axis), value)  64 us
    all_gather x1, waiting for transfers between devices, joined(): pieces = jax.tree.map(lambda part: lax.all_gather(part, axis), value)  26.5 us
    scatter x1, local copies, waits for them, and re-layouts, local(): new_cache = cache.at[seq_ids, target].set(new_rows, mode='drop')  25 us
    psum x1, waiting for transfers between devices, local(): sum_query, sum_latent = lax.psum((part_query, part_latent), 'kv')  18.9 us
    dot_general x1, matrix products, local(): jnp.einsum('sjc,skc->sjk', flat_query, cache, preferred_element_type=f32)  17.9 us
    dot_general x1, matrix products, local(): jnp.einsum('sjk,skc->sjc', weights.astype(bf16), cache[:, :, :latent_widt...  16.2 us
    add x7, other arithmetic, combine_totals(): numer_left * factor_left[..., None] + numer_right * factor_right[..., None]  10.2 us
  transfers between devices with their start and end apart: 3, of which 2 were waited for; matrix products, arithmetic and copies ran while one was open for 43% of the time, Pallas kernels for 0%

commit v1 on v0

v1 whole, which is shorter than its diff:
```python
import functools

import jax
import jax.numpy as jnp
from jax import lax
from jax.experimental import pallas as pl
from jax.experimental.pallas import tpu as pltpu
from jax.sharding import PartitionSpec as P

EPSILON = 1e-06
ROTARY_BASE = 10000.0
FLOOR_SCORE = -1e30
F32 = jnp.float32
BF16 = jnp.bfloat16


def exchange_kernel(axis, n, modes, *refs):
    count = len(modes)
    ins, outs = refs[:count], refs[count : 2 * count]
    send_sem, recv_sem, own_sem = refs[2 * count :]
    me = lax.axis_index(axis)
    barrier = pltpu.get_barrier_semaphore()
    for d in range(1, n):
        pl.semaphore_signal(
            barrier,
            inc=1,
            device_id={axis: lax.rem(me + d, n)},
            device_id_type=pl.DeviceIdType.MESH,
        )
    owns = []
    for a in range(count):
        src = ins[a] if modes[a] else ins[a].at[me]
        own = pltpu.make_async_copy(src, outs[a].at[me], own_sem.at[a])
        own.start()
        owns.append(own)
    pl.semaphore_wait(barrier, n - 1)
    copies = []
    for d in range(1, n):
        peer = lax.rem(me + d, n)
        for a in range(count):
            copy = pltpu.make_async_remote_copy(
                src_ref=ins[a] if modes[a] else ins[a].at[peer],
                dst_ref=outs[a].at[me],
                send_sem=send_sem.at[a, d],
                recv_sem=recv_sem.at[a, d],
                device_id={axis: peer},
                device_id_type=pl.DeviceIdType.MESH,
            )
            copy.start()
            copies.append(copy)
    for own in owns:
        own.wait()
    for copy in copies:
        copy.wait()


def exchange(arrays, modes, axis, n, cid):
    count = len(arrays)
    outs = [
        jax.ShapeDtypeStruct(((n,) + x.shape) if mode else x.shape, x.dtype)
        for x, mode in zip(arrays, modes)
    ]
    vmem = pl.BlockSpec(memory_space=pltpu.VMEM)
    return pl.pallas_call(
        functools.partial(exchange_kernel, axis, n, tuple(modes)),
        out_shape=outs,
        in_specs=[vmem] * count,
        out_specs=[vmem] * count,
        scratch_shapes=[
            pltpu.SemaphoreType.DMA((count, n)),
            pltpu.SemaphoreType.DMA((count, n)),
            pltpu.SemaphoreType.DMA((count,)),
        ],
        compiler_params=pltpu.CompilerParams(collective_id=cid, has_side_effects=True),
        name=f"exchange{cid}",
    )(*arrays)


def attend_kernel(ntp, nprop, latent, scale, meta, lengths, q_ref, new_ref, c_ref, o_ref, num_ref, md_ref):
    i = pl.program_id(0)
    tp = meta[0]
    offset = meta[1]
    groups = pl.num_programs(0) // ntp
    seq = lax.rem(lax.rem(i, ntp) + tp + 1, ntp) * groups + i // ntp
    span = c_ref.shape[2]
    start = lengths[seq] - offset
    o_ref[...] = c_ref[...]

    @pl.when((start > -nprop) & (start < span))
    def _():
        window = 256
        base = jnp.clip(start // 128 * 128, 0, span - window)
        base = pl.multiple_of(base, 128)
        rows = new_ref[0]
        slot = base + lax.broadcasted_iota(jnp.int32, (rows.shape[0], window), 1) - start
        which = lax.broadcasted_iota(jnp.int32, (rows.shape[0], window), 0)
        hot = ((slot == which) & (which < nprop)).astype(F32).astype(BF16)
        placed = lax.dot_general(
            rows, hot, (((0,), (0,)), ((), ())), preferred_element_type=F32
        )
        current = c_ref[0, :, pl.ds(base, window)].astype(F32)
        slot_all = base + lax.broadcasted_iota(jnp.int32, current.shape, 1) - start
        inside = (slot_all >= 0) & (slot_all < nprop)
        o_ref[0, :, pl.ds(base, window)] = jnp.where(inside, placed, current).astype(BF16)

    mine = lax.rem(i, ntp) == ntp - 1

    @pl.when(mine & (start > 0))
    def _():
        scores = jnp.dot(q_ref[0], c_ref[0], preferred_element_type=F32) * scale
        seen = lax.broadcasted_iota(jnp.int32, scores.shape, 1) < start
        masked = jnp.where(seen, scores, FLOOR_SCORE)
        peak = jnp.max(masked, axis=-1, keepdims=True)
        weights = jnp.where(seen, jnp.exp(masked - peak), 0.0)
        den = jnp.sum(weights, axis=-1, keepdims=True)
        num = lax.dot_general(
            weights.astype(BF16),
            c_ref[0, :latent, :],
            (((1,), (1,)), ((), ())),
            preferred_element_type=F32,
        )
        num_ref[0] = num.astype(BF16)
        lane = lax.broadcasted_iota(jnp.int32, (scores.shape[0], 128), 1)
        both = jnp.where(lane == 0, peak, den)
        md_ref[0] = jnp.transpose(both)[:8]

    @pl.when(mine & (start <= 0))
    def _():
        num_ref[...] = jnp.zeros_like(num_ref)
        which = lax.broadcasted_iota(jnp.int32, md_ref.shape[1:], 0)
        md_ref[0] = jnp.where(which == 0, FLOOR_SCORE, 0.0)


def attend(cache_t, queries, new_rows, lengths, meta, ntp, nprop, latent, scale):
    seqs, width, span = cache_t.shape
    groups, rows, _ = queries.shape

    def seq_of(i, meta):
        return lax.rem(lax.rem(i, ntp) + meta[0] + 1, ntp) * groups + i // ntp

    return pl.pallas_call(
        functools.partial(attend_kernel, ntp, nprop, latent, scale),
        grid_spec=pltpu.PrefetchScalarGridSpec(
            num_scalar_prefetch=2,
            grid=(seqs,),
            in_specs=[
                pl.BlockSpec((1, rows, width), lambda i, meta, lengths: (i // ntp, 0, 0)),
                pl.BlockSpec(
                    (1,) + new_rows.shape[1:], lambda i, meta, lengths: (seq_of(i, meta), 0, 0)
                ),
                pl.BlockSpec((1, width, span), lambda i, meta, lengths: (seq_of(i, meta), 0, 0)),
            ],
            out_specs=[
                pl.BlockSpec((1, width, span), lambda i, meta, lengths: (seq_of(i, meta), 0, 0)),
                pl.BlockSpec((1, rows, latent), lambda i, meta, lengths: (i // ntp, 0, 0)),
                pl.BlockSpec((1, 8, rows), lambda i, meta, lengths: (i // ntp, 0, 0)),
            ],
        ),
        out_shape=[
            jax.ShapeDtypeStruct(cache_t.shape, cache_t.dtype),
            jax.ShapeDtypeStruct((groups, rows, latent), BF16),
            jax.ShapeDtypeStruct((groups, 8, rows), F32),
        ],
        compiler_params=pltpu.CompilerParams(dimension_semantics=("arbitrary",)),
        name="attend",
    )(meta, lengths, queries, new_rows, cache_t)


def rms_scale(values, gain_vec):
    floats = values.astype(F32)
    return (
        floats
        * lax.rsqrt(jnp.mean(floats * floats, axis=-1, keepdims=True) + EPSILON)
        * gain_vec.astype(F32)
    )


def rotate(values, cosine, sine):
    half = values.shape[-1] // 2
    low, high = values[..., :half], values[..., half:]
    return jnp.concatenate([low * cosine - high * sine, low * sine + high * cosine], axis=-1)


def ancestor_bits(parents):
    masks = []
    for j in range(parents.shape[-1]):
        mask = jnp.full(parents.shape[:1], 1 << j, jnp.int32)
        for k in range(j):
            mask = mask | jnp.where(parents[:, j] == k, masks[k], 0)
        masks.append(mask)
    return jnp.stack(masks, axis=-1)


def pad_front(x, size):
    if x.shape[0] == size:
        return x
    return jnp.pad(x, [(0, size - x.shape[0])] + [(0, 0)] * (x.ndim - 1))


def local(
    nkv, ntp, tokens, in_gain, w_down_q, w_down_kv, w_rope_key, q_gain, kv_gain, w_up_q,
    w_absorb, w_value, w_out, out_gain, cache, cached, accepted, parents,
):
    seqs, nprop, model = tokens.shape
    down = w_down_q.shape[0]
    q_rank = w_down_q.shape[1]
    latent_w = w_down_kv.shape[1]
    rope_w = w_rope_key.shape[1]
    heads, nope = w_absorb.shape[:2]
    value_w = w_value.shape[1] // heads
    span = cache.shape[1]
    per_tp = seqs // ntp
    kv = lax.axis_index("kv")
    tp = lax.axis_index("tp")
    slot = jnp.minimum(kv, per_tp - 1)
    scale = (nope + rope_w) ** (-0.5)

    normed = rms_scale(tokens, in_gain).astype(BF16)
    own_seqs = lax.dynamic_slice_in_dim(normed, tp * per_tp, per_tp, 0)
    own_cols = lax.dynamic_slice_in_dim(own_seqs, kv * down, down, 2)
    w_down = jnp.concatenate([w_down_q, w_down_kv], axis=1)
    partial = jnp.dot(own_cols, w_down, preferred_element_type=F32)
    (parts,) = exchange([pad_front(partial, nkv)], [False], "kv", nkv, 1)
    sums = jnp.sum(parts, axis=0)
    query_in = rms_scale(sums[:, :q_rank], q_gain).astype(BF16)
    latent = rms_scale(sums[:, q_rank:], kv_gain).astype(BF16)
    query_in, latents = exchange([query_in, latent], [True, True], "tp", ntp, 2)

    lengths = cached + accepted
    bits = ancestor_bits(parents)
    positions = lengths[:, None] + lax.population_count(bits) - 1
    half = rope_w // 2
    frequency = ROTARY_BASE ** (-jnp.arange(half, dtype=F32) * 2.0 / rope_w)
    angles = positions.astype(F32)[..., None] * frequency
    cosine, sine = jnp.cos(angles), jnp.sin(angles)
    rope_key = rotate(
        jnp.dot(normed, w_rope_key, preferred_element_type=F32), cosine, sine
    ).astype(BF16)

    cos_own = lax.dynamic_index_in_dim(cosine.reshape(ntp, per_tp, nprop, half), slot, 1, False)
    sin_own = lax.dynamic_index_in_dim(sine.reshape(ntp, per_tp, nprop, half), slot, 1, False)
    queries = jnp.dot(query_in, w_up_q, preferred_element_type=F32).reshape(
        ntp, nprop, heads, nope + rope_w
    )
    query_rope = rotate(
        queries[..., nope:], cos_own[:, :, None], sin_own[:, :, None]
    ).astype(BF16)
    query_lat = jnp.einsum(
        "sphn,hnc->sphc", queries[..., :nope].astype(BF16), w_absorb, preferred_element_type=F32
    ).astype(BF16)
    full = jnp.concatenate([query_lat, query_rope], axis=-1).reshape(ntp, nprop * heads, -1)
    (full,) = exchange([full], [False], "tp", ntp, 3)
    rows = ntp * nprop * heads
    full = full.reshape(rows, latent_w + rope_w)
    all_queries, all_latents = exchange([full, latents], [True, True], "kv", nkv, 4)

    new_latents = all_latents[:per_tp].transpose(1, 0, 2, 3).reshape(seqs, nprop, latent_w)
    new_rows = jnp.concatenate([new_latents, rope_key], axis=-1)
    padded = jnp.pad(new_rows, ((0, 0), (0, -nprop % 16), (0, 0)))
    meta = jnp.stack([tp, kv * span]).astype(jnp.int32)
    cache_t, num, md = attend(
        cache.transpose(0, 2, 1), all_queries[:per_tp], padded, lengths, meta, ntp, nprop,
        latent_w, scale,
    )
    num, md = exchange(
        [pad_front(num, nkv), pad_front(md, nkv)], [False, False], "kv", nkv, 5
    )

    mine = tp * per_tp + slot
    my_rows = lax.dynamic_index_in_dim(new_rows, mine, 0, False)
    my_bits = lax.dynamic_index_in_dim(bits, mine, 0, False)
    row_prop = jnp.arange(rows) // heads % nprop
    row_bits = jnp.sum(
        jnp.where(row_prop[:, None] == jnp.arange(nprop)[None, :], my_bits[None, :], 0), axis=-1
    )
    allowed = ((row_bits[:, None] >> jnp.arange(nprop)[None, :]) & 1) == 1
    prop_scores = jnp.einsum("rc,kc->rk", full, my_rows, preferred_element_type=F32) * scale
    prop_masked = jnp.where(allowed, prop_scores, FLOOR_SCORE)
    prop_peak = jnp.max(prop_masked, axis=-1)
    prop_weights = jnp.where(allowed, jnp.exp(prop_masked - prop_peak[:, None]), 0.0)
    prop_den = jnp.sum(prop_weights, axis=-1)
    prop_num = jnp.dot(
        prop_weights.astype(BF16), my_rows[:, :latent_w], preferred_element_type=F32
    )
    peaks, dens = md[:, 0], md[:, 1]
    top = jnp.maximum(jnp.max(peaks, axis=0), prop_peak)
    factor = jnp.exp(peaks - top[None])
    prop_factor = jnp.exp(prop_peak - top)
    total_den = jnp.sum(factor * dens, axis=0) + prop_factor * prop_den
    total_num = jnp.sum(factor[..., None] * num.astype(F32), axis=0) + (
        prop_factor[:, None] * prop_num
    )
    lat_out = (total_num / total_den[:, None]).astype(BF16)
    (lat_out,) = exchange([lat_out.reshape(ntp, nprop * heads, latent_w)], [False], "tp", ntp, 6)
    head_out = jnp.einsum(
        "sphc,chv->sphv",
        lat_out.reshape(ntp, nprop, heads, latent_w),
        w_value.reshape(latent_w, heads, value_w),
        preferred_element_type=F32,
    ).astype(BF16)
    partials = jnp.dot(
        head_out.reshape(ntp, nprop, heads * value_w), w_out, preferred_element_type=F32
    ).astype(BF16)
    (partials,) = exchange([partials], [False], "tp", ntp, 7)
    summed = jnp.sum(partials.astype(F32), axis=0)
    attended = rms_scale(summed, out_gain).astype(BF16)
    (attended,) = exchange([attended], [True], "kv", nkv, 8)
    return attended[:per_tp], cache_t.transpose(0, 2, 1)


def solution(mesh):
    placed = (
        P(), P(), P("kv", None), P("kv", None), P(), P(), P(), P(None, "tp"),
        P("tp", None, None), P(None, "tp"), P("tp", None), P(), P(None, "kv", None), P(), P(), P(),
    )
    return jax.shard_map(
        functools.partial(local, mesh.shape["kv"], mesh.shape["tp"]),
        mesh=mesh,
        in_specs=placed,
        out_specs=(P("tp", None, None), P(None, "kv", None)),
        check_vma=False,
    )
```

time: 344 us -> 158 us (0.46)
  local copies, waits for them, and re-layouts: 148 us -> 9.77 us
  Pallas kernels: 0 us -> 123 us
  blocking collectives: 64 us -> 0 us
  waiting for transfers between devices: 45.5 us -> 0 us
  matrix products: 44.1 us -> 5.63 us
  between operations: 14.3 us -> 1.02 us
  other arithmetic: 24.2 us -> 16.4 us
    pallas_call x0 -> x9, Pallas kernels: none -> 123 us  [the longest x8 74.7 us: exchange(): pl.pallas_call(functools.partial(exchange_kernel, axis, n, tuple(modes)),...]
    unnamed x34 -> x25, local copies, waits for them, and re-layouts: 111 us -> 3.05 us
    all_gather x2 -> x0, blocking collectives: 64 us -> none  [joined(): pieces = jax.tree.map(lambda part: lax.all_gather(part, axis), value)]
    dot_general x11 -> x8, matrix products: 44.1 us -> 5.63 us  [the longest x1 1.03 us: local(): jnp.einsum('rc,kc->rk', full, my_rows, preferred_element_type=F32) * scale]
    all_gather x1 -> x0, waiting for transfers between devices: 26.5 us -> none  [joined(): pieces = jax.tree.map(lambda part: lax.all_gather(part, axis), value)]
    scatter x1 -> x0, local copies, waits for them, and re-layouts: 25 us -> none  [local(): new_cache = cache.at[seq_ids, target].set(new_rows, mode='drop')]
    psum x1 -> x0, waiting for transfers between devices: 18.9 us -> none  [local(): sum_query, sum_latent = lax.psum((part_query, part_latent), 'kv')]
    add x16 -> x1, other arithmetic: 10.4 us -> 0.01 us  [local(): total_den = jnp.sum(factor * dens, axis=0) + prop_factor * prop_den]
  transfers between devices with their start and end apart: 3 -> 0, of which waited for: 2 -> 0; matrix products, arithmetic and copies ran while one was open for 43% -> 0% of each run, Pallas kernels for 0% -> 0%
where the time goes in v1:
time: 158 us; the launch traced here: 156 us
  Pallas kernels  123 us (78%)
  other arithmetic  16.4 us (10%)
  local copies, waits for them, and re-layouts  9.77 us (6%)
  matrix products  5.63 us (4%)
    pallas_call x8, Pallas kernels, exchange(): pl.pallas_call(functools.partial(exchange_kernel, axis, n, tuple(modes)),...  74.7 us
    pallas_call x1, Pallas kernels, attend(): pl.pallas_call(functools.partial(attend_kernel, ntp, nprop, latent, scale...  48.7 us
    or x4, other arithmetic, ancestor_bits(): mask = mask | jnp.where(parents[:, j] == k, masks[k], 0)  3.53 us

profile of v1, /device:TPU:0, one launch (start us, length us, event | category | flops | bytes accessed | tf_op | source)
XLA Modules:
  0.0 156.2 jit_solution(12820720277393909839)
XLA Ops:
  0.7 0.6 pad_add_fusion.meta
  1.3 0.7 add.119.lengths
  2.0 0.7 convert_element_type.74
  2.7 0.1 add.126
  2.7 0.7 convert_element_type.72
  3.4 0.5 broadcast.352
  3.9 1.5 fusion.63
  5.5 0.7 reduce.21
  6.1 0.7 reduce.20
  6.8 0.7 reduce.19
  7.5 0.7 reduce.18
  8.2 0.2 dynamic-slice_reduce_fusion
  8.3 0.1 select_reduce_fusion
  8.4 0.1 stack.32
  8.9 1.4 fusion
  10.2 0.7 convert_element_type.70
  10.9 0.7 convert_element_type.87
  11.6 0.1 copy.76
  11.8 0.1 copy.71
  11.9 0.1 broadcast_multiply_fusion
  12.1 1.0 copy.80
  13.1 0.3 fusion.2
  13.4 0.1 constant_dynamic-slice_fusion
  13.5 0.7 fusion.24
  14.3 0.1 copy.96
  14.4 0.1 copy.95
  14.5 0.6 fusion.20
  15.1 0.9 fusion.10.refs_0_
  15.9 11.5 %exchange1.1 = f32[8,6,768]{2,1,0:T(8,128)} custom-call(f32[8,6,768]{2,1,0:T(8,128)} %fusion.10.refs_0_), custom_call_target="tpu_custom_call" | custom-call | tf_op jit(solution)/shard_map/exchange1/pallas_call | solution.py:64
  27.4 1.0 reduce_sum.91
  28.4 0.1 multiply_reduce_fusion.3
  28.5 0.1 multiply_reduce_fusion.2
  28.6 0.7 multiply_convert_fusion.2.refs_1_
  29.3 0.7 multiply_convert_fusion.1.refs_0_
  30.0 5.2 %exchange2.1 = (bf16[4,6,512]{2,1,0:T(8,128)(2,1)}, bf16[4,6,256]{2,1,0:T(8,128)(2,1)}) custom-call(bf16[6,512]{1,0:T(8,128)(2,1)} %multiply_convert_fusion.1.refs_0_, bf16[6,256]{1,0:T(8,128)(2,1)} %multiply_convert_fusion.2.refs_1_), custom_call_target="tpu_custom_call" | custom-call | tf_op jit(solution)/shard_map/exchange2/pallas_call | solution.py:64
  35.2 0.9 fusion.13
  36.1 0.1 reshape.215
  36.2 0.2 fusion.6
  36.4 0.1 fusion.70
  36.6 0.1 pad_maximum_fusion.1
  36.7 0.7 reshape.216.refs_0_
  37.4 5.4 %exchange3.1 = bf16[4,24,288]{2,1,0:T(8,128)(2,1)} custom-call(bf16[4,24,288]{2,1,0:T(8,128)(2,1)} %reshape.216.refs_0_), custom_call_target="tpu_custom_call" | custom-call | tf_op jit(solution)/shard_map/exchange3/pallas_call | solution.py:64
  42.8 18.7 %exchange4.1 = (bf16[8,96,288]{2,1,0:T(8,128)(2,1)}, bf16[8,4,6,256]{3,2,1,0:T(8,128)(2,1)}) custom-call(bf16[96,288]{1,0:T(8,128)(2,1)} %bitcast.59, bf16[4,6,256]{2,1,0:T(8,128)(2,1)} %get-tuple-element.12.refs_1_), custom_call_target="tpu_custom_call" | custom-call | tf_op jit(solution)/shard_map/exchange4/pallas_call | solution.py:64
  61.5 0.9 copy.74
  62.4 0.1 pad_maximum_fusion
  62.5 1.0 fusion.71
  63.6 0.8 pad.4.new_ref
  64.4 48.7 %attend.1 = (bf16[32,288,2048]{2,1,0:T(8,128)(2,1)}, bf16[8,96,256]{2,1,0:T(8,128)(2,1)}, f32[8,8,96]{2,1,0:T(8,128)}) custom-call(s32[2]{0:T(128)} %pad_add_fusion.meta, s32[32]{0:T(128)} %copy-done.5, bf16[8,96,288]{2,1,0:T(8,128)(2,1)} %get-tuple-element.13.q_ref, bf16[32,16,288]{2,1,0:T(8,128)(2,1)} %pad.4.new_ref, bf16[32,288,2048]{2,1,0:T(8,128)(2,1)} %bitcast.58), custom_call_target="tpu_custom_call" | custom-call | tf_op jit(solution)/shard_map/attend/pallas_call | solution.py:141
  113.1 11.9 %exchange5.1 = (bf16[8,96,256]{2,1,0:T(8,128)(2,1)}, f32[8,8,96]{2,1,0:T(8,128)}) custom-call(bf16[8,96,256]{2,1,0:T(8,128)(2,1)} %get-tuple-element.15.refs_0_, f32[8,8,96]{2,1,0:T(8,128)} %get-tuple-element.16.refs_1_), custom_call_target="tpu_custom_call" | custom-call | tf_op jit(solution)/shard_map/exchange5/pallas_call | solution.py:64
  125.0 0.8 slice.73
  125.7 0.8 copy.79
  126.6 1.2 multiply_reduce_fusion
  127.8 0.8 fusion.5
  128.6 5.2 %exchange6.1 = bf16[4,24,256]{2,1,0:T(8,128)(2,1)} custom-call(bf16[4,24,256]{2,1,0:T(8,128)(2,1)} %bitcast.64), custom_call_target="tpu_custom_call" | custom-call | tf_op jit(solution)/shard_map/exchange6/pallas_call | solution.py:64
  133.8 0.8 reshape.220
  134.6 0.2 fusion.7
  134.8 0.1 reshape.229
  134.9 0.9 convolution_convert_fusion.refs_0_
  135.8 5.7 %exchange7.1 = bf16[4,6,2048]{2,1,0:T(8,128)(2,1)} custom-call(bf16[4,6,2048]{2,1,0:T(8,128)(2,1)} %convolution_convert_fusion.refs_0_), custom_call_target="tpu_custom_call" | custom-call | tf_op jit(solution)/shard_map/exchange7/pallas_call | solution.py:64
  141.5 0.9 convert_reduce_fusion
  142.5 0.1 multiply_reduce_fusion.1
  142.6 0.7 multiply_convert_fusion.refs_0_
  143.3 11.2 %exchange8.1 = bf16[8,6,2048]{2,1,0:T(8,128)(2,1)} custom-call(bf16[6,2048]{1,0:T(8,128)(2,1)} %multiply_convert_fusion.refs_0_), custom_call_target="tpu_custom_call" | custom-call | tf_op jit(solution)/shard_map/exchange8/pallas_call | solution.py:64
  154.5 1.7 %copy.84 = bf16[8,6,2048]{2,0,1:T(8,128)(2,1)} copy(bf16[8,6,2048]{2,1,0:T(8,128)(2,1)} %exchange8.1) | data formatting | bytes 393216
  (47 shorter events, 0.8 us)
Async XLA Ops:
  0.6 134.3 %copy-start = (bf16[256,2048]{1,0:T(8,128)(2,1)S(1)}, bf16[256,2048]{1,0:T(8,128)(2,1)}, u32[]{:S(2)}) copy-start(bf16[256,2048]{1,0:T(8,128)(2,1)} %param.26) | copy-start | bytes 3145732
  0.6 12.4 %copy-start.1 = (bf16[32,6,2048]{2,0,1:T(8,128)(2,1)S(1)}, bf16[32,6,2048]{2,0,1:T(8,128)(2,1)}, u32[]{:S(2)}) copy-start(bf16[32,6,2048]{2,0,1:T(8,128)(2,1)} %param.16) | copy-start | bytes 2359300
  0.7 12.8 %copy-start.4 = (bf16[2048,32]{0,1:T(8,128)(2,1)S(1)}, bf16[2048,32]{0,1:T(8,128)(2,1)}, u32[]{:S(2)}) copy-start(bf16[2048,32]{0,1:T(8,128)(2,1)} %param.20) | copy-start | bytes 393220
  2.0 12.2 %copy-start.5 = (s32[32]{0:T(128)}, s32[32]{0:T(128)S(1)}, u32[]{:S(2)}) copy-start(s32[32]{0:T(128)S(1)} %add.119.lengths) | copy-start | bytes 388
  13.1 2.0 %copy-start.6 = (bf16[256,512]{1,0:T(8,128)(2,1)S(1)}, bf16[256,512]{1,0:T(8,128)(2,1)}, u32[]{:S(2)}) copy-start(bf16[256,512]{1,0:T(8,128)(2,1)} %param.18) | copy-start | bytes 786436
  13.1 2.0 %copy-start.7 = (bf16[256,256]{1,0:T(8,128)(2,1)S(1)}, bf16[256,256]{1,0:T(8,128)(2,1)}, u32[]{:S(2)}) copy-start(bf16[256,256]{1,0:T(8,128)(2,1)} %param.19) | copy-start | bytes 393220
  13.5 21.7 %copy-start.2 = (bf16[512,384]{1,0:T(8,128)(2,1)S(1)}, bf16[512,384]{1,0:T(8,128)(2,1)}, u32[]{:S(2)}) copy-start(bf16[512,384]{1,0:T(8,128)(2,1)} %param.23) | copy-start | bytes 1179652
  14.2 22.0 %copy-start.3 = (bf16[4,64,256]{2,1,0:T(8,128)(2,1)S(1)}, bf16[4,64,256]{2,1,0:T(8,128)(2,1)}, u32[]{:S(2)}) copy-start(bf16[4,64,256]{2,1,0:T(8,128)(2,1)} %param.24) | copy-start | bytes 393220

commit v2 on v1

--- a/solution.py
+++ b/solution.py
@@ -80,34 +80,35 @@
     i = pl.program_id(0)
     tp = meta[0]
     offset = meta[1]
-    groups = pl.num_programs(0) // ntp
-    seq = lax.rem(lax.rem(i, ntp) + tp + 1, ntp) * groups + i // ntp
-    span = c_ref.shape[2]
-    start = lengths[seq] - offset
+    groups = pl.num_programs(0)
+    span = c_ref.shape[3]
     o_ref[...] = c_ref[...]
 
-    @pl.when((start > -nprop) & (start < span))
+    for g in range(ntp):
+        begin = lengths[g * groups + i] - offset
+
+        @pl.when((begin > -nprop) & (begin < span))
+        def _(g=g, begin=begin):
+            window = 256
+            base = jnp.clip(begin // 128 * 128, 0, span - window)
+            base = pl.multiple_of(base, 128)
+            rows = new_ref[g, 0]
+            slot = base + lax.broadcasted_iota(jnp.int32, (rows.shape[0], window), 1) - begin
+            which = lax.broadcasted_iota(jnp.int32, (rows.shape[0], window), 0)
+            hot = ((slot == which) & (which < nprop)).astype(F32).astype(BF16)
+            placed = lax.dot_general(
+                rows, hot, (((0,), (0,)), ((), ())), preferred_element_type=F32
+            )
+            current = c_ref[g, 0, :, pl.ds(base, window)].astype(F32)
+            slot_all = base + lax.broadcasted_iota(jnp.int32, current.shape, 1) - begin
+            inside = (slot_all >= 0) & (slot_all < nprop)
+            o_ref[g, 0, :, pl.ds(base, window)] = jnp.where(inside, placed, current).astype(BF16)
+
+    start = lengths[tp * groups + i] - offset
+
+    @pl.when(start > 0)
     def _():
-        window = 256
-        base = jnp.clip(start // 128 * 128, 0, span - window)
-        base = pl.multiple_of(base, 128)
-        rows = new_ref[0]
-        slot = base + lax.broadcasted_iota(jnp.int32, (rows.shape[0], window), 1) - start
-        which = lax.broadcasted_iota(jnp.int32, (rows.shape[0], window), 0)
-        hot = ((slot == which) & (which < nprop)).astype(F32).astype(BF16)
-        placed = lax.dot_general(
-            rows, hot, (((0,), (0,)), ((), ())), preferred_element_type=F32
-        )
-        current = c_ref[0, :, pl.ds(base, window)].astype(F32)
-        slot_all = base + lax.broadcasted_iota(jnp.int32, current.shape, 1) - start
-        inside = (slot_all >= 0) & (slot_all < nprop)
-        o_ref[0, :, pl.ds(base, window)] = jnp.where(inside, placed, current).astype(BF16)
-
-    mine = lax.rem(i, ntp) == ntp - 1
-
-    @pl.when(mine & (start > 0))
-    def _():
-        scores = jnp.dot(q_ref[0], c_ref[0], preferred_element_type=F32) * scale
+        scores = jnp.dot(q_ref[0], c_ref[tp, 0], preferred_element_type=F32) * scale
         seen = lax.broadcasted_iota(jnp.int32, scores.shape, 1) < start
         masked = jnp.where(seen, scores, FLOOR_SCORE)
         peak = jnp.max(masked, axis=-1, keepdims=True)
@@ -115,7 +116,7 @@
         den = jnp.sum(weights, axis=-1, keepdims=True)
         num = lax.dot_general(
             weights.astype(BF16),
-            c_ref[0, :latent, :],
+            c_ref[tp, 0, :latent, :],
             (((1,), (1,)), ((), ())),
             preferred_element_type=F32,
         )
@@ -124,7 +125,7 @@
         both = jnp.where(lane == 0, peak, den)
         md_ref[0] = jnp.transpose(both)[:8]
 
-    @pl.when(mine & (start <= 0))
+    @pl.when(start <= 0)
     def _():
         num_ref[...] = jnp.zeros_like(num_ref)
         which = lax.broadcasted_iota(jnp.int32, md_ref.shape[1:], 0)
@@ -134,36 +135,34 @@
 def attend(cache_t, queries, new_rows, lengths, meta, ntp, nprop, latent, scale):
     seqs, width, span = cache_t.shape
     groups, rows, _ = queries.shape
-
-    def seq_of(i, meta):
-        return lax.rem(lax.rem(i, ntp) + meta[0] + 1, ntp) * groups + i // ntp
-
+    cache_g = cache_t.reshape(ntp, groups, width, span)
+    new_g = new_rows.reshape((ntp, groups) + new_rows.shape[1:])
     return pl.pallas_call(
         functools.partial(attend_kernel, ntp, nprop, latent, scale),
         grid_spec=pltpu.PrefetchScalarGridSpec(
             num_scalar_prefetch=2,
-            grid=(seqs,),
+            grid=(groups,),
             in_specs=[
-                pl.BlockSpec((1, rows, width), lambda i, meta, lengths: (i // ntp, 0, 0)),
+                pl.BlockSpec((1, rows, width), lambda i, meta, lengths: (i, 0, 0)),
                 pl.BlockSpec(
-                    (1,) + new_rows.shape[1:], lambda i, meta, lengths: (seq_of(i, meta), 0, 0)
+                    (ntp, 1) + new_g.shape[2:], lambda i, meta, lengths: (0, i, 0, 0)
                 ),
-                pl.BlockSpec((1, width, span), lambda i, meta, lengths: (seq_of(i, meta), 0, 0)),
+                pl.BlockSpec((ntp, 1, width, span), lambda i, meta, lengths: (0, i, 0, 0)),
             ],
             out_specs=[
-                pl.BlockSpec((1, width, span), lambda i, meta, lengths: (seq_of(i, meta), 0, 0)),
-                pl.BlockSpec((1, rows, latent), lambda i, meta, lengths: (i // ntp, 0, 0)),
-                pl.BlockSpec((1, 8, rows), lambda i, meta, lengths: (i // ntp, 0, 0)),
+                pl.BlockSpec((ntp, 1, width, span), lambda i, meta, lengths: (0, i, 0, 0)),
+                pl.BlockSpec((1, rows, latent), lambda i, meta, lengths: (i, 0, 0)),
+                pl.BlockSpec((1, 8, rows), lambda i, meta, lengths: (i, 0, 0)),
             ],
         ),
         out_shape=[
-            jax.ShapeDtypeStruct(cache_t.shape, cache_t.dtype),
+            jax.ShapeDtypeStruct(cache_g.shape, cache_t.dtype),
             jax.ShapeDtypeStruct((groups, rows, latent), BF16),
             jax.ShapeDtypeStruct((groups, 8, rows), F32),
         ],
         compiler_params=pltpu.CompilerParams(dimension_semantics=("arbitrary",)),
         name="attend",
-    )(meta, lengths, queries, new_rows, cache_t)
+    )(meta, lengths, queries, new_g, cache_g)
 
 
 def rms_scale(values, gain_vec):
@@ -305,7 +304,7 @@
     summed = jnp.sum(partials.astype(F32), axis=0)
     attended = rms_scale(summed, out_gain).astype(BF16)
     (attended,) = exchange([attended], [True], "kv", nkv, 8)
-    return attended[:per_tp], cache_t.transpose(0, 2, 1)
+    return attended[:per_tp], cache_t.reshape(seqs, -1, span).transpose(0, 2, 1)
 
 
 def solution(mesh):

time: 158 us -> 142 us (0.90)
  Pallas kernels: 123 us -> 108 us
    pallas_call x1, Pallas kernels: 48.7 us -> 33.1 us  [attend(): pl.pallas_call(functools.partial(attend_kernel, ntp, nprop, latent, scale...]
where the time goes in v2:
time: 142 us; the launch traced here: 141 us
  Pallas kernels  108 us (76%)
  other arithmetic  16.1 us (11%)
  local copies, waits for them, and re-layouts  9.82 us (7%)
  matrix products  5.63 us (4%)
    pallas_call x8, Pallas kernels, exchange(): pl.pallas_call(functools.partial(exchange_kernel, axis, n, tuple(modes)),...  75.3 us
    pallas_call x1, Pallas kernels, attend(): pl.pallas_call(functools.partial(attend_kernel, ntp, nprop, latent, scale...  33.1 us
    or x4, other arithmetic, ancestor_bits(): mask = mask | jnp.where(parents[:, j] == k, masks[k], 0)  3.53 us
    unnamed x25, local copies, waits for them, and re-layouts  2.94 us

profile of v2, /device:TPU:0, one launch (start us, length us, event | category | flops | bytes accessed | tf_op | source)
XLA Modules:
  0.0 141.0 jit_solution(11073470121953751762)
XLA Ops:
  0.7 0.6 pad_add_fusion.meta
  1.3 0.7 add.119.lengths
  2.0 0.7 convert_element_type.74
  2.7 0.1 add.126
  2.7 0.7 convert_element_type.72
  3.4 0.5 broadcast.352
  3.9 1.5 %fusion.63 = (s32[32]{0:T(128)S(1)}, s32[32,1]{0,1:T(1,128)S(1)}, s32[32,1]{0,1:T(1,128)S(1)}, s32[32,1]{0,1:T(1,128)S(1)}, s32[32,1]{0,1:T(1,128)S(1)}, /*index=5*/s32[32,1]{0,1:T(1,128)S(1)}) fusion(s32[]{:T(128)} %broadcast.352, s32[32,6]{0,1:T(8,128)} %param.31), kind=kLoop, calls=%fused_computation.137 | loop fusion | flops 1440 | bytes 1412 | tf_op jit(solution)/shard_map/or | solution.py:188
  5.5 0.7 reduce.21
  6.1 0.7 reduce.20
  6.8 0.7 reduce.19
  7.5 0.7 reduce.18
  8.2 0.2 dynamic-slice_reduce_fusion
  8.3 0.1 select_reduce_fusion
  8.4 0.1 stack.32
  8.5 0.1 stack.33
  8.9 1.4 fusion
  10.2 0.7 convert_element_type.70
  10.9 0.7 convert_element_type.87
  11.7 0.1 copy.86
  11.8 0.1 broadcast_multiply_fusion
  12.0 1.1 copy.94
  13.1 0.3 fusion.2
  13.3 0.1 constant_dynamic-slice_fusion.1
  13.5 0.7 fusion.16
  14.2 0.3 fusion.28
  14.5 0.1 copy.90
  14.6 0.1 copy.91
  14.7 0.9 fusion.10.refs_0_
  15.6 11.5 %exchange1.1 = f32[8,6,768]{2,1,0:T(8,128)} custom-call(f32[8,6,768]{2,1,0:T(8,128)} %fusion.10.refs_0_), custom_call_target="tpu_custom_call" | custom-call | tf_op jit(solution)/shard_map/exchange1/pallas_call | solution.py:64
  27.1 1.0 reduce_sum.91
  28.0 0.1 multiply_reduce_fusion.3
  28.1 0.1 multiply_reduce_fusion.2
  28.3 0.7 multiply_convert_fusion.2.refs_1_
  28.9 0.7 multiply_convert_fusion.1.refs_0_
  29.6 5.2 %exchange2.1 = (bf16[4,6,512]{2,1,0:T(8,128)(2,1)}, bf16[4,6,256]{2,1,0:T(8,128)(2,1)}) custom-call(bf16[6,512]{1,0:T(8,128)(2,1)} %multiply_convert_fusion.1.refs_0_, bf16[6,256]{1,0:T(8,128)(2,1)} %multiply_convert_fusion.2.refs_1_), custom_call_target="tpu_custom_call" | custom-call | tf_op jit(solution)/shard_map/exchange2/pallas_call | solution.py:64
  34.8 0.9 fusion.13
  35.7 0.1 reshape.224
  35.9 0.2 fusion.6
  36.0 0.1 fusion.69
  36.2 0.1 pad_maximum_fusion.1
  36.3 0.7 reshape.225.refs_0_
  37.0 5.4 %exchange3.1 = bf16[4,24,288]{2,1,0:T(8,128)(2,1)} custom-call(bf16[4,24,288]{2,1,0:T(8,128)(2,1)} %reshape.225.refs_0_), custom_call_target="tpu_custom_call" | custom-call | tf_op jit(solution)/shard_map/exchange3/pallas_call | solution.py:64
  42.4 18.7 %exchange4.1 = (bf16[8,96,288]{2,1,0:T(8,128)(2,1)}, bf16[8,4,6,256]{3,2,1,0:T(8,128)(2,1)}) custom-call(bf16[96,288]{1,0:T(8,128)(2,1)} %bitcast.68, bf16[4,6,256]{2,1,0:T(8,128)(2,1)} %get-tuple-element.12.refs_1_), custom_call_target="tpu_custom_call" | custom-call | tf_op jit(solution)/shard_map/exchange4/pallas_call | solution.py:64
  61.1 1.0 copy.143
  62.1 0.1 pad_maximum_fusion
  62.2 1.0 fusion.70
  63.3 0.8 pad.4.clone
  64.1 33.1 %attend.1 = (bf16[4,8,288,2048]{3,2,1,0:T(8,128)(2,1)}, bf16[8,96,256]{2,1,0:T(8,128)(2,1)}, f32[8,8,96]{2,1,0:T(8,128)}) custom-call(s32[2]{0:T(128)} %pad_add_fusion.meta, s32[32]{0:T(128)} %copy-done.5, bf16[8,96,288]{2,1,0:T(8,128)(2,1)} %get-tuple-element.13.q_ref, bf16[4,8,16,288]{3,2,1,0:T(8,128)(2,1)} %bitcast.67, bf16[4,8,288,2048]{3,2,1,0:T(8,128)(2,1)} %bitcast.66), custom_call_target="tpu_custom_call" | custom-call | tf_op jit(solution)/shard_map/attend/pallas_call | solution.py:140
  97.3 12.5 %exchange5.1 = (bf16[8,96,256]{2,1,0:T(8,128)(2,1)}, f32[8,8,96]{2,1,0:T(8,128)}) custom-call(bf16[8,96,256]{2,1,0:T(8,128)(2,1)} %get-tuple-element.15.refs_0_, f32[8,8,96]{2,1,0:T(8,128)} %get-tuple-element.16.refs_1_), custom_call_target="tpu_custom_call" | custom-call | tf_op jit(solution)/shard_map/exchange5/pallas_call | solution.py:64
  109.7 0.8 slice.73
  110.5 0.8 copy.93
  111.3 1.2 multiply_reduce_fusion
  112.5 0.8 fusion.5
  113.4 5.2 %exchange6.1 = bf16[4,24,256]{2,1,0:T(8,128)(2,1)} custom-call(bf16[4,24,256]{2,1,0:T(8,128)(2,1)} %bitcast.73), custom_call_target="tpu_custom_call" | custom-call | tf_op jit(solution)/shard_map/exchange6/pallas_call | solution.py:64
  118.6 0.8 reshape.231
  119.4 0.2 fusion.7
  119.6 0.1 reshape.241
  119.7 0.9 convolution_convert_fusion.refs_0_
  120.6 5.7 %exchange7.1 = bf16[4,6,2048]{2,1,0:T(8,128)(2,1)} custom-call(bf16[4,6,2048]{2,1,0:T(8,128)(2,1)} %convolution_convert_fusion.refs_0_), custom_call_target="tpu_custom_call" | custom-call | tf_op jit(solution)/shard_map/exchange7/pallas_call | solution.py:64
  126.2 0.9 convert_reduce_fusion
  127.2 0.1 multiply_reduce_fusion.1
  127.3 0.7 multiply_convert_fusion.refs_0_
  128.0 11.2 %exchange8.1 = bf16[8,6,2048]{2,1,0:T(8,128)(2,1)} custom-call(bf16[6,2048]{1,0:T(8,128)(2,1)} %multiply_convert_fusion.refs_0_), custom_call_target="tpu_custom_call" | custom-call | tf_op jit(solution)/shard_map/exchange8/pallas_call | solution.py:64
  139.2 1.7 %copy.98 = bf16[8,6,2048]{2,0,1:T(8,128)(2,1)} copy(bf16[8,6,2048]{2,1,0:T(8,128)(2,1)} %exchange8.1) | data formatting | bytes 393216
  (47 shorter events, 0.8 us)
Async XLA Ops:
  0.6 119.0 %copy-start = (bf16[256,2048]{1,0:T(8,128)(2,1)S(1)}, bf16[256,2048]{1,0:T(8,128)(2,1)}, u32[]{:S(2)}) copy-start(bf16[256,2048]{1,0:T(8,128)(2,1)} %param.26) | copy-start | bytes 3145732
  0.6 12.4 %copy-start.1 = (bf16[32,6,2048]{2,0,1:T(8,128)(2,1)S(1)}, bf16[32,6,2048]{2,0,1:T(8,128)(2,1)}, u32[]{:S(2)}) copy-start(bf16[32,6,2048]{2,0,1:T(8,128)(2,1)} %param.16) | copy-start | bytes 2359300
  0.7 12.8 %copy-start.4 = (bf16[2048,32]{0,1:T(8,128)(2,1)S(1)}, bf16[2048,32]{0,1:T(8,128)(2,1)}, u32[]{:S(2)}) copy-start(bf16[2048,32]{0,1:T(8,128)(2,1)} %param.20) | copy-start | bytes 393220
  2.0 12.2 %copy-start.5 = (s32[32]{0:T(128)}, s32[32]{0:T(128)S(1)}, u32[]{:S(2)}) copy-start(s32[32]{0:T(128)S(1)} %add.119.lengths) | copy-start | bytes 388
  12.0 2.7 %copy-start.6 = (bf16[256,512]{1,0:T(8,128)(2,1)S(1)}, bf16[256,512]{1,0:T(8,128)(2,1)}, u32[]{:S(2)}) copy-start(bf16[256,512]{1,0:T(8,128)(2,1)} %param.18) | copy-start | bytes 786436
  12.0 2.7 %copy-start.7 = (bf16[256,256]{1,0:T(8,128)(2,1)S(1)}, bf16[256,256]{1,0:T(8,128)(2,1)}, u32[]{:S(2)}) copy-start(bf16[256,256]{1,0:T(8,128)(2,1)} %param.19) | copy-start | bytes 393220
  13.3 21.5 %copy-start.2 = (bf16[512,384]{1,0:T(8,128)(2,1)S(1)}, bf16[512,384]{1,0:T(8,128)(2,1)}, u32[]{:S(2)}) copy-start(bf16[512,384]{1,0:T(8,128)(2,1)} %param.23) | copy-start | bytes 1179652
  13.4 22.4 %copy-start.3 = (bf16[4,64,256]{2,1,0:T(8,128)(2,1)S(1)}, bf16[4,64,256]{2,1,0:T(8,128)(2,1)}, u32[]{:S(2)}) copy-start(bf16[4,64,256]{2,1,0:T(8,128)(2,1)} %param.24) | copy-start | bytes 393220
